TPU v7x, 32 devices: a whole 2x2x4 slice. The times are simulated.
32 devices in a mesh: sp: 4 (over z), fs: 4 (over y, x), tp: 2 (over core).
Axes of the slice: x: 2, y: 2, z: 4, core: 2. Of those that a mesh axis runs over, the one named last changes fastest.
Arguments:
- tokens: bfloat16 [4, 640, 2048], P('fs', 'sp', 'tp'), may hold values from -6 to 6
- mix_gain: float32 [2048], replicated, may hold values from 0.1 to 1.9
- conv_b_weight: bfloat16 [2048, 1024], P(('sp', 'fs'), 'tp'), may hold values from -0.125 to 0.125
- conv_c_weight: bfloat16 [2048, 1024], P(('sp', 'fs'), 'tp'), may hold values from -0.125 to 0.125
- conv_v_weight: bfloat16 [2048, 1024], P(('sp', 'fs'), 'tp'), may hold values from -0.125 to 0.125
- conv_taps: float32 [3, 1024], P(None, 'tp'), may hold values from -3.5 to 3.5
- query_weight: bfloat16 [2048, 2048], P(('sp', 'fs'), 'tp'), may hold values from -0.125 to 0.125
- query_rope_weight: bfloat16 [2048, 1024], P(('sp', 'fs'), 'tp'), may hold values from -4.5 to 4.5
- latent_weight: bfloat16 [2048, 512], P(('sp', 'fs')), may hold values from -0.125 to 0.125
- key_rope_weight: bfloat16 [2048, 64], replicated, may hold values from -1 to 1
- latent_gain: float32 [512], replicated, may hold values from 0.1 to 1.9
- key_up_weight: bfloat16 [512, 2048], P(None, 'tp'), may hold values from -0.25 to 0.25
- value_up_weight: bfloat16 [512, 2048], P(None, 'tp'), may hold values from -0.25 to 0.25
- head_gain: float32 [2048], P('tp'), may hold values from 0.1 to 1.9
- conv_out_weight: bfloat16 [1024, 2048], P('tp', ('sp', 'fs')), may hold values from -0.109375 to 0.109375
- attn_out_weight: bfloat16 [2048, 2048], P('tp', ('sp', 'fs')), may hold values from -0.109375 to 0.109375
Outputs:
- mixed: bfloat16 [4, 640, 2048], P('fs', ('sp', 'tp'))
All inputs are finite; a program needn't handle non-finite values.
Results may differ from a plain program's by a relative error of at most 0.025.
Values may be sent and summed in bfloat16 or wider, within the bound.
No kernel may reach another device: no remote copies, remote signals or barrier semaphores. Data moves between devices by JAX's collectives and lax.ppermute only.
A program may use at most 128 MiB of HBM per device.

v0:
```python
import jax
import jax.numpy as jnp
from jax import lax
from jax.sharding import PartitionSpec as P

NOPE = 128
ROPE = 64
VD = 128
KVL = 512
SEG = 64
norm_epsilon = 1e-06
rope_theta = 10000.0


def passed_along(block, axis, distance):
    devices = range(lax.axis_size(axis))
    route = [(i - distance, i) for i in devices if i - distance in devices]
    return lax.ppermute(block, axis, route)


def rms_scale(values, gain):
    return (
        values * lax.rsqrt(jnp.mean(values * values, axis=-1, keepdims=True) + norm_epsilon) * gain
    )


def rope_tables(positions):
    half_width = ROPE // 2
    frequency = rope_theta ** (-jnp.arange(half_width, dtype=jnp.float32) * 2.0 / ROPE)
    angles = positions[:, None] * frequency[None, :]
    return (jnp.cos(angles), jnp.sin(angles))


def rotate(values, cosine, sine):
    half_width = ROPE // 2
    first = values[..., :half_width]
    second = values[..., half_width:]
    return jnp.concatenate(
        [first * cosine - second * sine, second * cosine + first * sine], axis=-1
    )


def shards(
    tokens,
    mix_gain,
    conv_b_weight,
    conv_c_weight,
    conv_v_weight,
    conv_taps,
    query_weight,
    query_rope_weight,
    latent_weight,
    key_rope_weight,
    latent_gain,
    key_up_weight,
    value_up_weight,
    head_gain,
    conv_out_weight,
    attn_out_weight,
):
    full_rows = lax.all_gather(tokens[0], "tp", axis=1, tiled=True)
    tok_rows = full_rows.shape[0]
    normed = rms_scale(full_rows.astype(jnp.float32), mix_gain).astype(jnp.bfloat16)
    offset = lax.axis_index("sp") * tok_rows
    token_index = offset + jnp.arange(tok_rows, dtype=jnp.int32)
    cosine, sine = rope_tables(token_index.astype(jnp.float32))
    local_heads = query_weight.shape[1] // NOPE
    count_sp = lax.axis_size("sp")
    count_fs = lax.axis_size("fs")
    count_tp = lax.axis_size("tp")
    fs_index = lax.axis_index("fs")
    row_piece = normed.shape[1] // (count_sp * count_fs)
    all_normed = lax.all_gather(normed, "fs", axis=0, tiled=True)
    picked = lax.dynamic_index_in_dim(
        all_normed.reshape(-1, count_sp, count_fs, row_piece), fs_index, 2, keepdims=False
    ).reshape(-1, count_sp * row_piece)
    gathered = (
        lax.all_gather(conv_b_weight, "sp", axis=0, tiled=True),
        lax.all_gather(conv_c_weight, "sp", axis=0, tiled=True),
        lax.all_gather(conv_v_weight, "sp", axis=0, tiled=True),
        lax.all_gather(query_weight, "sp", axis=0, tiled=True),
        lax.all_gather(query_rope_weight, "sp", axis=0, tiled=True),
        lax.all_gather(latent_weight, "sp", axis=0, tiled=True),
    )

    def project_in():
        return jnp.concatenate(
            [jnp.dot(picked, member, preferred_element_type=jnp.float32) for member in gathered],
            axis=1,
        )

    joined = lax.psum_scatter(
        project_in().astype(jnp.bfloat16), "fs", scatter_dimension=0, tiled=True
    ).astype(jnp.float32)
    bounds = []
    running_total = 0
    for member in gathered[:-1]:
        running_total = running_total + member.shape[1]
        bounds.append(running_total)
    sums = tuple(jnp.split(joined, bounds, axis=1))
    latent_raw = sums[5].astype(jnp.bfloat16)
    gate_b = sums[0].astype(jnp.bfloat16)
    gate_c = sums[1].astype(jnp.bfloat16)
    values_v = sums[2].astype(jnp.bfloat16)
    query_nope = sums[3].astype(jnp.bfloat16).reshape(tok_rows, local_heads, NOPE)
    query_rot = rotate(
        sums[4].reshape(tok_rows, local_heads, ROPE), cosine[:, None, :], sine[:, None, :]
    ).astype(jnp.bfloat16)
    latent = rms_scale(latent_raw.astype(jnp.float32), latent_gain).astype(jnp.bfloat16)
    key_rot = rotate(
        jnp.dot(normed, key_rope_weight, preferred_element_type=jnp.float32), cosine, sine
    ).astype(jnp.bfloat16)
    query_latent = jnp.einsum(
        "thn,khn->thk",
        query_nope,
        key_up_weight.reshape(KVL, local_heads, NOPE),
        preferred_element_type=jnp.float32,
    ).astype(jnp.bfloat16)
    attn_scale = (NOPE + ROPE) ** (-0.5)
    product = (gate_c.astype(jnp.float32) * values_v.astype(jnp.float32)).astype(jnp.bfloat16)
    previous = passed_along(product[tok_rows - 2 :], "sp", 1)
    padded = jnp.concatenate([previous, product], axis=0).astype(jnp.float32)
    convolved = (
        conv_taps[0] * padded[0:tok_rows]
        + conv_taps[1] * padded[1 : tok_rows + 1]
        + conv_taps[2] * padded[2 : tok_rows + 2]
    )
    conv_y = (gate_b.astype(jnp.float32) * convolved).astype(jnp.bfloat16)
    query_segment = token_index // SEG
    last_segment = (offset + tok_rows - 1) // SEG

    def key_block(running, latent_block, rot_block, first_key):
        peak_old, denom_old, accum_old = running
        block_rows = latent_block.shape[0]
        scores = (
            jnp.einsum(
                "thk,jk->thj", query_latent, latent_block, preferred_element_type=jnp.float32
            )
            + jnp.einsum("thr,jr->thj", query_rot, rot_block, preferred_element_type=jnp.float32)
        ) * attn_scale
        key_segment = (first_key + jnp.arange(block_rows, dtype=jnp.int32)) // SEG
        allowed = key_segment[None, None, :] <= query_segment[:, None, None]
        peak_new = jnp.maximum(peak_old, jnp.max(jnp.where(allowed, scores, -1e30), axis=-1))
        weights = jnp.where(allowed, jnp.exp(scores - peak_new[..., None]), 0.0)
        rescale = jnp.exp(peak_old - peak_new)
        denom_new = denom_old * rescale + jnp.sum(weights, axis=-1)
        accum_new = accum_old * rescale[..., None] + jnp.einsum(
            "thj,jk->thk",
            weights.astype(jnp.bfloat16),
            latent_block,
            preferred_element_type=jnp.float32,
        )
        return (peak_new, denom_new, accum_new)

    starting = (
        jnp.full((tok_rows, local_heads), -1e30, jnp.float32),
        jnp.zeros((tok_rows, local_heads), jnp.float32),
        jnp.zeros((tok_rows, local_heads, KVL), jnp.float32),
    )
    latent_piece = lax.all_gather(latent, "sp", axis=0, tiled=True)
    rot_piece = lax.all_gather(key_rot, "sp", axis=0, tiled=True)
    piece_rows = latent_piece.shape[0]
    splits = max(1, piece_rows // 512)
    while piece_rows % splits:
        splits = splits - 1
    block_rows = piece_rows // splits

    def visit(state, block_index):
        block_begin = block_index * block_rows
        latent_block = lax.dynamic_slice_in_dim(latent_piece, block_begin, block_rows, 0)
        rot_block = lax.dynamic_slice_in_dim(rot_piece, block_begin, block_rows, 0)
        updated = lax.cond(
            block_begin // SEG <= last_segment,
            lambda inner: key_block(inner, latent_block, rot_block, block_begin),
            lambda inner: inner,
            state,
        )
        return (updated, None)

    peak, denom, accum = lax.scan(visit, starting, jnp.arange(splits, dtype=jnp.int32))[0]
    attended = (accum / denom[..., None]).astype(jnp.bfloat16)
    head_out = jnp.einsum(
        "thk,khv->thv",
        attended,
        value_up_weight.reshape(KVL, local_heads, VD),
        preferred_element_type=jnp.float32,
    )
    normed_heads = rms_scale(head_out, head_gain.reshape(local_heads, VD))
    attn_y = normed_heads.astype(jnp.bfloat16).reshape(tok_rows, local_heads * VD)
    share_rows = tok_rows // count_tp
    conv_all, attn_all = (
        lax.all_gather(conv_y, "fs", axis=0, tiled=True),
        lax.all_gather(attn_y, "fs", axis=0, tiled=True),
    )
    conv_sorted = (
        conv_all.reshape(count_fs, count_tp, share_rows, -1)
        .transpose(1, 0, 2, 3)
        .reshape(count_fs * tok_rows, -1)
    )
    attn_sorted = (
        attn_all.reshape(count_fs, count_tp, share_rows, -1)
        .transpose(1, 0, 2, 3)
        .reshape(count_fs * tok_rows, -1)
    )
    conv_cols_sp, attn_cols_sp = (
        lax.all_gather(conv_out_weight, "sp", axis=1, tiled=True),
        lax.all_gather(attn_out_weight, "sp", axis=1, tiled=True),
    )
    col_sums = lax.psum_scatter(
        (
            jnp.dot(conv_sorted, conv_cols_sp, preferred_element_type=jnp.float32)
            + jnp.dot(attn_sorted, attn_cols_sp, preferred_element_type=jnp.float32)
        ).astype(jnp.bfloat16),
        "tp",
        scatter_dimension=0,
        tiled=True,
    )
    col_piece = conv_cols_sp.shape[1] // count_sp
    outgoing = col_sums.reshape(count_fs, share_rows, count_sp * col_piece)
    arrived = lax.all_to_all(outgoing, "fs", split_axis=0, concat_axis=2, tiled=True)
    result = (
        arrived.reshape(share_rows, count_fs, count_sp, col_piece)
        .transpose(0, 2, 1, 3)
        .reshape(share_rows, count_fs * count_sp * col_piece)
    )
    return result[None]


def solution(mesh):
    return jax.shard_map(
        shards,
        mesh=mesh,
        in_specs=(
            P("fs", "sp", "tp"),
            P(),
            P(("sp", "fs"), "tp"),
            P(("sp", "fs"), "tp"),
            P(("sp", "fs"), "tp"),
            P(None, "tp"),
            P(("sp", "fs"), "tp"),
            P(("sp", "fs"), "tp"),
            P(("sp", "fs"), None),
            P(),
            P(),
            P(None, "tp"),
            P(None, "tp"),
            P("tp"),
            P("tp", ("sp", "fs")),
            P("tp", ("sp", "fs")),
        ),
        out_specs=P("fs", ("sp", "tp"), None),
        check_vma=False,
    )
```

profile of v0, /device:TPU:0, one launch (start us, length us, event | category | flops | bytes accessed | tf_op | source)
XLA Modules:
  0.0 311.9 jit_solution(16413146177102707444)
XLA Ops:
  6.6 2.7 all-gather
  9.5 1.8 fusion.22
  12.2 17.5 %all_gather.44 = bf16[512,512]{1,0:T(8,128)(2,1)S(1)} all-gather(bf16[128,512]{1,0:T(8,128)(2,1)S(1)} %copy-done.9), channel_id=1, replica_groups=mesh['sp'=4,'fs'=4,'tp'=2] {'sp'}, dimensions={0}, use_global_device_ids=true | all-gather | bytes 655360 | tf_op jit(solution)/shard_map/all_gather | solution.py:78
  29.6 16.5 %all_gather.45 = bf16[512,512]{1,0:T(8,128)(2,1)} all-gather(bf16[128,512]{1,0:T(8,128)(2,1)S(1)} %copy-done.10), channel_id=1, replica_groups=mesh['sp'=4,'fs'=4,'tp'=2] {'sp'}, dimensions={0}, use_global_device_ids=true | all-gather | bytes 655360 | tf_op jit(solution)/shard_map/all_gather | solution.py:79
  46.1 16.7 %all_gather.46 = bf16[512,512]{1,0:T(8,128)(2,1)} all-gather(bf16[128,512]{1,0:T(8,128)(2,1)S(1)} %copy-done.11), channel_id=1, replica_groups=mesh['sp'=4,'fs'=4,'tp'=2] {'sp'}, dimensions={0}, use_global_device_ids=true | all-gather | bytes 655360 | tf_op jit(solution)/shard_map/all_gather | solution.py:80
  62.8 22.8 %all_gather.48 = bf16[512,512]{1,0:T(8,128)(2,1)S(1)} all-gather(bf16[128,512]{1,0:T(8,128)(2,1)S(1)} %copy-done.12), channel_id=1, replica_groups=mesh['sp'=4,'fs'=4,'tp'=2] {'sp'}, dimensions={0}, use_global_device_ids=true | all-gather | bytes 655360 | tf_op jit(solution)/shard_map/all_gather | solution.py:82
  85.6 17.8 %all_gather.49 = bf16[512,512]{1,0:T(8,128)(2,1)} all-gather(bf16[128,512]{1,0:T(8,128)(2,1)S(1)} %copy-done.13), channel_id=1, replica_groups=mesh['sp'=4,'fs'=4,'tp'=2] {'sp'}, dimensions={0}, use_global_device_ids=true | all-gather | bytes 655360 | tf_op jit(solution)/shard_map/all_gather | solution.py:83
  103.4 4.4 %copy.65 = bf16[640,2048]{0,1:T(8,128)(2,1)} copy(bf16[640,2048]{1,0:T(8,128)(2,1)} %all-gather.7.cloned.1.call-done) | data formatting | bytes 5242880 | tf_op jit(solution)/shard_map/all_gather | solution.py:73
  109.9 2.5 convolution_convert_fusion.5
  113.8 2.5 convolution_convert_fusion.4
  120.4 3.3 %fusion.15 = bf16[640,3584]{1,0:T(8,128)(2,1)} fusion(bf16[640,3584]{1,0:T(8,128)(2,1)} %constant_dynamic-update-slice_fusion, bf16[640,512]{0,1:T(8,128)(2,1)S(1)} %bitcast.104, bf16[512,1024]{1,0:T(8,128)(2,1)} %all-gather.9.cloned.1.call-done), kind=kOutput, calls=%fused_computation.35 | convolution fusion | flops 671744000 | bytes 3014656 | tf_op jit(solution)/shard_map/dot_general | solution.py:88
  128.4 1.9 broadcast_in_dim.56
  130.3 14.1 %all-gather.1 = bf16[4,160,64]{1,2,0:T(8,128)(2,1)} all-gather(bf16[1,160,64]{1,2,0:T(8,128)(2,1)S(1)} %maximum_bitcast_fusion), channel_id=1, replica_groups=mesh['sp'=4,'fs'=4,'tp'=2] {'sp'}, dimensions={0}, use_global_device_ids=true | all-gather | bytes 102400 | tf_op jit(solution)/shard_map/all_gather | solution.py:161
  144.3 36.4 %reduce-scatter.3.cloned.1.call-done = bf16[160,3584]{1,0:T(8,128)(2,1)} async-done(((bf16[640,3584]{1,0:T(8,128)(2,1)}), bf16[160,3584]{1,0:T(8,128)(2,1)}) %reduce-scatter.3.cloned.1.call-update) | async-done | bytes 1146896 | tf_op jit(solution)/shard_map/reduce_scatter | solution.py:92
  181.8 1.8 fusion.34
  183.6 17.8 %all_gather.52 = bf16[640,512]{1,0:T(8,128)(2,1)S(1)} all-gather(bf16[160,512]{1,0:T(8,128)(2,1)S(1)} %get-tuple-element.251), channel_id=1, replica_groups=mesh['sp'=4,'fs'=4,'tp'=2] {'sp'}, dimensions={0}, use_global_device_ids=true | all-gather | bytes 819200 | tf_op jit(solution)/shard_map/all_gather | solution.py:160
  203.0 1.5 fusion.16
  204.5 12.2 %conditional.1 = ((f32[160,8]{1,0:T(8,128)S(1)}, f32[160,8,512]{2,1,0:T(8,128)})) conditional(s32[]{:T(128)} %convert_element_type.79, (f32[160,8]{1,0:T(8,128)S(1)}, f32[160,8,512]{2,1,0:T(8,128)}) %tuple.31, (s32[160]{0:T(256)S(1)}, s32[160]{0:T(256)S(1)}, s32[]{:T(128)}, bf16[160,8,512]{2,0,1:T(8,128)(2,1)S(1)}, ...), branch_computations={%region_3.4_spmd, %region_4.7_spmd.clone} | conditional | flops 1792195712 | bytes 46272084 | solution.py:172
  204.9 1.7 copy.85
  206.5 1.7 reshape.204
  209.7 1.9 select_reduce_fusion
  213.3 1.8 multiply_add_fusion
  215.1 1.5 copy-done.2
  216.7 2.1 divide_convert_fusion
  221.6 2.5 collective-permute-start
  224.1 15.4 %all_gather.51 = bf16[512,512]{1,0:T(8,128)(2,1)S(1)} all-gather(bf16[512,128]{1,0:T(8,128)(2,1)S(1)} %copy-done.14), channel_id=1, replica_groups=mesh['sp'=4,'fs'=4,'tp'=2] {'sp'}, dimensions={1}, use_global_device_ids=true | all-gather | bytes 655360 | tf_op jit(solution)/shard_map/all_gather | solution.py:206
  240.6 12.5 %all_gather.50 = bf16[640,512]{1,0:T(8,128)(2,1)S(1)} all-gather(bf16[160,512]{1,0:T(8,128)(2,1)S(1)} %fusion.40), channel_id=1, replica_groups=mesh['sp'=4,'fs'=4,'tp'=2] {'fs'}, dimensions={0}, use_global_device_ids=true | all-gather | bytes 819200 | tf_op jit(solution)/shard_map/all_gather | solution.py:192
  253.6 2.5 copy.81
  256.1 26.6 %all-gather.13.cloned.1.call-done = bf16[1024,512]{1,0:T(8,128)(2,1)} async-done(((bf16[1024,128]{1,0:T(8,128)(2,1)}), bf16[1024,512]{1,0:T(8,128)(2,1)}) %all-gather.13.cloned.1.call-update) | async-done | bytes 1048592 | tf_op jit(solution)/shard_map/all_gather | solution.py:207
  282.8 3.3 %fusion.17 = bf16[640,512]{1,0:T(8,128)(2,1)} fusion(f32[640,512]{1,0:T(8,128)S(1)} %fusion.44, bf16[640,1024]{1,0:T(8,128)(2,1)} %bitcast.98, bf16[1024,512]{1,0:T(8,128)(2,1)} %all-gather.13.cloned.1.call-done), kind=kOutput, calls=%fused_computation.38 | convolution fusion | flops 671744000 | bytes 4325376 | tf_op jit(solution)/shard_map/dot_general | solution.py:212
  286.1 6.5 %reduce-scatter.5.cloned.1.call-done = bf16[320,512]{1,0:T(8,128)(2,1)} async-done(((bf16[640,512]{1,0:T(8,128)(2,1)}), bf16[320,512]{1,0:T(8,128)(2,1)}) %reduce-scatter.5.cloned.1.call-update) | async-done | bytes 327696 | tf_op jit(solution)/shard_map/reduce_scatter | solution.py:209
  292.6 11.0 %all_to_all.15 = bf16[4,80,512]{2,1,0:T(8,128)(2,1)S(1)} all-to-all(bf16[4,80,512]{2,1,0:T(8,128)(2,1)} %bitcast.107), channel_id=1, replica_groups=mesh['sp'=4,'fs'=4,'tp'=2] {'fs'}, dimensions={0} | all-to-all | bytes 655360 | tf_op jit(solution)/shard_map/all_to_all | solution.py:220
  (99 shorter events, 25.0 us)
Async XLA Ops:
  6.5 196.5 %copy-start = (bf16[512,1024]{1,0:T(8,128)(2,1)S(1)}, bf16[512,1024]{1,0:T(8,128)(2,1)}, u32[]{:S(2)}) copy-start(bf16[512,1024]{1,0:T(8,128)(2,1)} %param.29) | copy-start | bytes 3145732
  6.5 5.6 %copy-start.9 = (bf16[128,512]{1,0:T(8,128)(2,1)S(1)}, bf16[128,512]{1,0:T(8,128)(2,1)}, u32[]{:S(2)}) copy-start(bf16[128,512]{1,0:T(8,128)(2,1)} %param.20) | copy-start | bytes 393220
  6.5 23.1 %copy-start.10 = (bf16[128,512]{1,0:T(8,128)(2,1)S(1)}, bf16[128,512]{1,0:T(8,128)(2,1)}, u32[]{:S(2)}) copy-start(bf16[128,512]{1,0:T(8,128)(2,1)} %param.21) | copy-start | bytes 393220
  6.5 39.6 %copy-start.11 = (bf16[128,512]{1,0:T(8,128)(2,1)S(1)}, bf16[128,512]{1,0:T(8,128)(2,1)}, u32[]{:S(2)}) copy-start(bf16[128,512]{1,0:T(8,128)(2,1)} %param.22) | copy-start | bytes 393220
  6.5 96.9 %all-gather.7.cloned.1.call-start = ((), (), s32[]{:S(2)}) async-start(), calls=%async_computation.3 | async-start | bytes 3276800 | tf_op jit(solution)/shard_map/all_gather | solution.py:73
  9.3 53.5 %copy-start.12 = (bf16[128,512]{1,0:T(8,128)(2,1)S(1)}, bf16[128,512]{1,0:T(8,128)(2,1)}, u32[]{:S(2)}) copy-start(bf16[128,512]{1,0:T(8,128)(2,1)} %param.25) | copy-start | bytes 393220
  9.3 76.3 %copy-start.13 = (bf16[128,512]{1,0:T(8,128)(2,1)S(1)}, bf16[128,512]{1,0:T(8,128)(2,1)}, u32[]{:S(2)}) copy-start(bf16[128,512]{1,0:T(8,128)(2,1)} %param.26) | copy-start | bytes 393220
  11.4 109.0 %all-gather.9.cloned.1.call-start = ((), (), s32[]{:S(2)}) async-start(), calls=%async_computation.4 | async-start | bytes 1310720 | tf_op jit(solution)/shard_map/all_gather | solution.py:81
  12.1 168.6 %reduce-scatter.3.cloned.1.call-start = ((), (), s32[]{:S(2)}) async-start(), calls=%async_computation.5 | async-start | bytes 5734400 | tf_op jit(solution)/shard_map/reduce_scatter | solution.py:92
  109.0 4.8 %copy-start.5 = (bf16[640,4,1,128]{0,3,2,1:T(8,128)(2,1)}, bf16[640,4,1,128]{0,3,2,1:T(8,128)(2,1)S(1)}, u32[]{:S(2)}) copy-start(bf16[640,4,1,128]{0,3,2,1:T(8,128)(2,1)S(1)} %constant_dynamic-slice_fusion) | copy-start | bytes 1966084
  118.5 1.8 copy-start.6
  120.4 4.7 %copy-start.7 = (bf16[512,512]{1,0:T(8,128)(2,1)S(1)}, bf16[512,512]{1,0:T(8,128)(2,1)}, u32[]{:S(2)}) copy-start(bf16[512,512]{1,0:T(8,128)(2,1)} %all_gather.49) | copy-start | bytes 1572868
  126.5 1.1 copy-start.3
  126.5 1.1 copy-start.8
  126.5 55.3 %copy-start.17 = (f32[512]{0:T(512)S(1)}, f32[512]{0:T(512)}, u32[]{:S(2)}) copy-start(f32[512]{0:T(512)} %param.28) | copy-start | bytes 6148
  126.5 127.1 %all-gather.11.cloned.1.call-start = ((), (), s32[]{:S(2)}) async-start(), calls=%async_computation.6 | async-start | bytes 1638400 | tf_op jit(solution)/shard_map/all_gather | solution.py:193
  211.6 1.7 copy-start.1
  215.1 1.5 copy-start.2
  216.7 2.1 copy-start.18
  218.8 1.1 copy-start.16
  218.8 2.8 copy-start.15
  218.8 2.8 copy-start.4
  218.8 5.3 %copy-start.14 = (bf16[512,128]{1,0:T(8,128)(2,1)S(1)}, bf16[512,128]{1,0:T(8,128)(2,1)}, u32[]{:S(2)}) copy-start(bf16[512,128]{1,0:T(8,128)(2,1)} %param.32) | copy-start | bytes 393220
  220.9 61.9 %all-gather.13.cloned.1.call-start = ((), (), s32[]{:S(2)}) async-start(), calls=%async_computation.7 | async-start | bytes 1310720 | tf_op jit(solution)/shard_map/all_gather | solution.py:207
  221.5 71.1 %reduce-scatter.5.cloned.1.call-start = ((), (), s32[]{:S(2)}) async-start(), calls=%async_computation.8 | async-start | bytes 983040 | tf_op jit(solution)/shard_map/reduce_scatter | solution.py:209
  221.6 17.9 %collective-permute-start = (bf16[2,512]{1,0:T(2,128)(2,1)S(1)}, bf16[2,512]{1,0:T(2,128)(2,1)S(1)}, u32[]{:S(2)}, u32[]{:S(2)}) collective-permute-start(bf16[2,512]{1,0:T(2,128)(2,1)S(1)} %slice.44), channel_id=1, source_target_pairs={{0,8},{8,16},{16,24},{1,9},{9,17},{17,25},{2,10},{10,18},{18,26},{... | collective-permute-start | bytes 6152 | tf_op jit(solution)/shard_map/ppermute | solution.py:18
Sparse Core Ops, SparseCore 0:
  11.5 42.1 all-gather.6
  55.2 39.4 all-gather.8
  126.6 54.0 reduce-scatter.2
  221.0 30.3 all-gather.10
  252.8 29.8 all-gather.12
  286.2 6.3 reduce-scatter.4
where the time goes:
time: 313 us; the launch traced here: 312 us
  blocking collectives  165 us (53%)
  waiting for transfers between devices  70.9 us (23%)
  local copies, waits for them, and re-layouts  23.9 us (8%)
  matrix products  23.6 us (8%)
  between operations  13.8 us (4%)
  other arithmetic  12 us (4%)
    reduce_scatter x1, waiting for transfers between devices, shards(): lax.psum_scatter(project_in().astype(jnp.bfloat16), 'fs', scatter_dimensi...  36.4 us
    all_gather x1, waiting for transfers between devices, shards(): lax.all_gather(attn_out_weight, 'sp', axis=1, tiled=True)  26.6 us
    all_gather x1, blocking collectives, shards(): lax.all_gather(query_rope_weight, 'sp', axis=0, tiled=True)  22.8 us
    all_gather x1, blocking collectives, shards(): lax.all_gather(latent_weight, 'sp', axis=0, tiled=True)  17.8 us
    all_gather x1, blocking collectives, shards(): latent_piece = lax.all_gather(latent, 'sp', axis=0, tiled=True)  17.8 us
    all_gather x1, blocking collectives, shards(): lax.all_gather(conv_b_weight, 'sp', axis=0, tiled=True)  17.5 us
    all_gather x1, blocking collectives, shards(): lax.all_gather(conv_v_weight, 'sp', axis=0, tiled=True)  16.7 us
    all_gather x1, blocking collectives, shards(): lax.all_gather(conv_c_weight, 'sp', axis=0, tiled=True)  16.5 us
  transfers between devices with their start and end apart: 7, of which 3 were waited for; matrix products, arithmetic and copies ran while one was open for 8% of the time, Pallas kernels for 0%

commit v1 on v0

--- a/solution.py
+++ b/solution.py
@@ -157,8 +157,11 @@
         jnp.zeros((tok_rows, local_heads), jnp.float32),
         jnp.zeros((tok_rows, local_heads, KVL), jnp.float32),
     )
-    latent_piece = lax.all_gather(latent, "sp", axis=0, tiled=True)
-    rot_piece = lax.all_gather(key_rot, "sp", axis=0, tiled=True)
+    latent_piece, rot_piece = jnp.split(
+        lax.all_gather(jnp.concatenate([latent, key_rot], axis=1), "sp", axis=0, tiled=True),
+        [latent.shape[1]],
+        axis=1,
+    )
     piece_rows = latent_piece.shape[0]
     splits = max(1, piece_rows // 512)
     while piece_rows % splits:

time: 313 us -> 313 us (level)
  waiting for transfers between devices: 70.9 us -> 86.3 us
  blocking collectives: 165 us -> 153 us
  local copies, waits for them, and re-layouts: 23.9 us -> 20.7 us
    reduce_scatter x1, waiting for transfers between devices: 36.4 us -> 51.5 us  [shards(): lax.psum_scatter(project_in().astype(jnp.bfloat16), 'fs', scatter_dimensi...]
    all_gather x2 -> x1, blocking collectives: 31.9 us -> 19.9 us  [shards(): lax.all_gather(jnp.concatenate([latent, key_rot], axis=1), 'sp', axis=0,...]
where the time goes in v1:
time: 313 us; the launch traced here: 312 us
  blocking collectives  153 us (49%)
  waiting for transfers between devices  86.3 us (28%)
  matrix products  23.8 us (8%)
  local copies, waits for them, and re-layouts  20.7 us (7%)
  between operations  13.8 us (4%)
  other arithmetic  12.4 us (4%)
    reduce_scatter x1, waiting for transfers between devices, shards(): lax.psum_scatter(project_in().astype(jnp.bfloat16), 'fs', scatter_dimensi...  51.5 us
    all_gather x1, waiting for transfers between devices, shards(): lax.all_gather(attn_out_weight, 'sp', axis=1, tiled=True)  27 us
    all_gather x1, blocking collectives, shards(): lax.all_gather(query_rope_weight, 'sp', axis=0, tiled=True)  22.8 us
    all_gather x1, blocking collectives, shards(): lax.all_gather(jnp.concatenate([latent, key_rot], axis=1), 'sp', axis=0,...  19.9 us
    all_gather x1, blocking collectives, shards(): lax.all_gather(latent_weight, 'sp', axis=0, tiled=True)  17.8 us
    all_gather x1, blocking collectives, shards(): lax.all_gather(conv_b_weight, 'sp', axis=0, tiled=True)  17.5 us
    all_gather x1, blocking collectives, shards(): lax.all_gather(conv_v_weight, 'sp', axis=0, tiled=True)  16.7 us
    all_gather x1, blocking collectives, shards(): lax.all_gather(conv_c_weight, 'sp', axis=0, tiled=True)  16.5 us
  transfers between devices with their start and end apart: 7, of which 3 were waited for; matrix products, arithmetic and copies ran while one was open for 8% of the time, Pallas kernels for 0%

profile of v1, /device:TPU:0, one launch (start us, length us, event | category | flops | bytes accessed | tf_op | source)
XLA Modules:
  0.0 311.9 jit_solution(18355218734900224190)
XLA Ops:
  6.6 2.7 all-gather
  9.5 1.8 fusion.23
  12.2 17.5 %all_gather.41 = bf16[512,512]{1,0:T(8,128)(2,1)S(1)} all-gather(bf16[128,512]{1,0:T(8,128)(2,1)S(1)} %copy-done.8), channel_id=1, replica_groups=mesh['sp'=4,'fs'=4,'tp'=2] {'sp'}, dimensions={0}, use_global_device_ids=true | all-gather | bytes 655360 | tf_op jit(solution)/shard_map/all_gather | solution.py:78
  29.6 16.5 %all_gather.42 = bf16[512,512]{1,0:T(8,128)(2,1)} all-gather(bf16[128,512]{1,0:T(8,128)(2,1)S(1)} %copy-done.9), channel_id=1, replica_groups=mesh['sp'=4,'fs'=4,'tp'=2] {'sp'}, dimensions={0}, use_global_device_ids=true | all-gather | bytes 655360 | tf_op jit(solution)/shard_map/all_gather | solution.py:79
  46.1 16.7 %all_gather.43 = bf16[512,512]{1,0:T(8,128)(2,1)} all-gather(bf16[128,512]{1,0:T(8,128)(2,1)S(1)} %copy-done.10), channel_id=1, replica_groups=mesh['sp'=4,'fs'=4,'tp'=2] {'sp'}, dimensions={0}, use_global_device_ids=true | all-gather | bytes 655360 | tf_op jit(solution)/shard_map/all_gather | solution.py:80
  62.8 22.8 %all_gather.45 = bf16[512,512]{1,0:T(8,128)(2,1)S(1)} all-gather(bf16[128,512]{1,0:T(8,128)(2,1)S(1)} %copy-done.11), channel_id=1, replica_groups=mesh['sp'=4,'fs'=4,'tp'=2] {'sp'}, dimensions={0}, use_global_device_ids=true | all-gather | bytes 655360 | tf_op jit(solution)/shard_map/all_gather | solution.py:82
  85.6 17.8 %all_gather.46 = bf16[512,512]{1,0:T(8,128)(2,1)} all-gather(bf16[128,512]{1,0:T(8,128)(2,1)S(1)} %copy-done.12), channel_id=1, replica_groups=mesh['sp'=4,'fs'=4,'tp'=2] {'sp'}, dimensions={0}, use_global_device_ids=true | all-gather | bytes 655360 | tf_op jit(solution)/shard_map/all_gather | solution.py:83
  103.4 4.5 %copy.67 = bf16[640,2048]{0,1:T(8,128)(2,1)} copy(bf16[640,2048]{1,0:T(8,128)(2,1)} %all-gather.6.cloned.1.call-done) | data formatting | bytes 5242880 | tf_op jit(solution)/shard_map/all_gather | solution.py:73
  109.9 2.5 convolution_convert_fusion.5
  112.4 1.3 copy.71
  113.8 2.5 convolution_convert_fusion.4
  120.4 3.3 %fusion.16 = bf16[640,3584]{1,0:T(8,128)(2,1)} fusion(bf16[640,3584]{1,0:T(8,128)(2,1)} %constant_dynamic-update-slice_fusion, bf16[640,512]{0,1:T(8,128)(2,1)S(1)} %bitcast.100, bf16[512,1024]{1,0:T(8,128)(2,1)} %all-gather.8.cloned.1.call-done), kind=kOutput, calls=%fused_computation.37 | convolution fusion | flops 671744000 | bytes 3014656 | tf_op jit(solution)/shard_map/dot_general | solution.py:88
  123.7 1.4 fusion.20
  125.1 1.4 fusion.19
  126.7 1.9 broadcast_in_dim.56
  129.3 51.5 %reduce-scatter.3.cloned.1.call-done = bf16[160,3584]{1,0:T(8,128)(2,1)} async-done(((bf16[640,3584]{1,0:T(8,128)(2,1)}), bf16[160,3584]{1,0:T(8,128)(2,1)}) %reduce-scatter.3.cloned.1.call-update) | async-done | bytes 1146896 | tf_op jit(solution)/shard_map/reduce_scatter | solution.py:92
  183.2 19.9 %all_gather.49 = bf16[640,576]{1,0:T(8,128)(2,1)S(1)} all-gather(bf16[160,576]{1,0:T(8,128)(2,1)S(1)} %pad_maximum_fusion.1), channel_id=1, replica_groups=mesh['sp'=4,'fs'=4,'tp'=2] {'sp'}, dimensions={0}, use_global_device_ids=true | all-gather | bytes 921600 | tf_op jit(solution)/shard_map/all_gather | solution.py:161
  205.4 1.5 fusion.17
  206.9 10.1 %conditional.1 = ((f32[160,8]{1,0:T(8,128)S(1)}, f32[160,8,512]{2,1,0:T(8,128)})) conditional(s32[]{:T(128)} %convert_element_type.79, (f32[160,8]{1,0:T(8,128)S(1)}, f32[160,8,512]{2,1,0:T(8,128)}) %tuple.31, (s32[160]{0:T(256)S(1)}, s32[160]{0:T(256)S(1)}, s32[]{:T(128)}, bf16[640,576]{1,0:T(8,128)(2,1)S(1)}, ...), branch_computations={%region_3.4_spmd, %region_4.7_spmd.clone} | conditional | flops 1792195712 | bytes 47736404 | solution.py:175
  208.4 1.5 fusion.11
  210.0 1.9 select_reduce_fusion
  213.6 1.8 multiply_add_fusion
  215.4 1.6 copy-done.2
  217.0 2.1 divide_convert_fusion
  222.0 1.5 collective-permute-start
  223.5 14.3 %all_gather.48 = bf16[512,512]{1,0:T(8,128)(2,1)S(1)} all-gather(bf16[512,128]{1,0:T(8,128)(2,1)S(1)} %copy-done.13), channel_id=1, replica_groups=mesh['sp'=4,'fs'=4,'tp'=2] {'sp'}, dimensions={1}, use_global_device_ids=true | all-gather | bytes 655360 | tf_op jit(solution)/shard_map/all_gather | solution.py:209
  239.0 13.8 %all_gather.47 = bf16[640,512]{1,0:T(8,128)(2,1)S(1)} all-gather(bf16[160,512]{1,0:T(8,128)(2,1)S(1)} %fusion.41), channel_id=1, replica_groups=mesh['sp'=4,'fs'=4,'tp'=2] {'fs'}, dimensions={0}, use_global_device_ids=true | all-gather | bytes 819200 | tf_op jit(solution)/shard_map/all_gather | solution.py:195
  253.3 2.5 copy.82
  255.8 27.0 %all-gather.12.cloned.1.call-done = bf16[1024,512]{1,0:T(8,128)(2,1)} async-done(((bf16[1024,128]{1,0:T(8,128)(2,1)}), bf16[1024,512]{1,0:T(8,128)(2,1)}) %all-gather.12.cloned.1.call-update) | async-done | bytes 1048592 | tf_op jit(solution)/shard_map/all_gather | solution.py:210
  282.8 3.3 %fusion.18 = bf16[640,512]{1,0:T(8,128)(2,1)} fusion(f32[640,512]{1,0:T(8,128)S(1)} %fusion.45, bf16[640,1024]{1,0:T(8,128)(2,1)} %bitcast.94, bf16[1024,512]{1,0:T(8,128)(2,1)} %all-gather.12.cloned.1.call-done), kind=kOutput, calls=%fused_computation.40 | convolution fusion | flops 671744000 | bytes 4325376 | tf_op jit(solution)/shard_map/dot_general | solution.py:215
  286.1 6.5 %reduce-scatter.5.cloned.1.call-done = bf16[320,512]{1,0:T(8,128)(2,1)} async-done(((bf16[640,512]{1,0:T(8,128)(2,1)}), bf16[320,512]{1,0:T(8,128)(2,1)}) %reduce-scatter.5.cloned.1.call-update) | async-done | bytes 327696 | tf_op jit(solution)/shard_map/reduce_scatter | solution.py:212
  292.6 11.0 %all_to_all.15 = bf16[4,80,512]{2,1,0:T(8,128)(2,1)S(1)} all-to-all(bf16[4,80,512]{2,1,0:T(8,128)(2,1)} %bitcast.103), channel_id=1, replica_groups=mesh['sp'=4,'fs'=4,'tp'=2] {'fs'}, dimensions={0} | all-to-all | bytes 655360 | tf_op jit(solution)/shard_map/all_to_all | solution.py:223
  (93 shorter events, 21.6 us)
Async XLA Ops:
  6.5 198.9 %copy-start = (bf16[512,1024]{1,0:T(8,128)(2,1)S(1)}, bf16[512,1024]{1,0:T(8,128)(2,1)}, u32[]{:S(2)}) copy-start(bf16[512,1024]{1,0:T(8,128)(2,1)} %param.29) | copy-start | bytes 3145732
  6.5 5.6 %copy-start.8 = (bf16[128,512]{1,0:T(8,128)(2,1)S(1)}, bf16[128,512]{1,0:T(8,128)(2,1)}, u32[]{:S(2)}) copy-start(bf16[128,512]{1,0:T(8,128)(2,1)} %param.20) | copy-start | bytes 393220
  6.5 23.1 %copy-start.9 = (bf16[128,512]{1,0:T(8,128)(2,1)S(1)}, bf16[128,512]{1,0:T(8,128)(2,1)}, u32[]{:S(2)}) copy-start(bf16[128,512]{1,0:T(8,128)(2,1)} %param.21) | copy-start | bytes 393220
  6.5 39.6 %copy-start.10 = (bf16[128,512]{1,0:T(8,128)(2,1)S(1)}, bf16[128,512]{1,0:T(8,128)(2,1)}, u32[]{:S(2)}) copy-start(bf16[128,512]{1,0:T(8,128)(2,1)} %param.22) | copy-start | bytes 393220
  6.5 96.9 %all-gather.6.cloned.1.call-start = ((), (), s32[]{:S(2)}) async-start(), calls=%async_computation.3 | async-start | bytes 3276800 | tf_op jit(solution)/shard_map/all_gather | solution.py:73
  9.3 53.5 %copy-start.11 = (bf16[128,512]{1,0:T(8,128)(2,1)S(1)}, bf16[128,512]{1,0:T(8,128)(2,1)}, u32[]{:S(2)}) copy-start(bf16[128,512]{1,0:T(8,128)(2,1)} %param.25) | copy-start | bytes 393220
  9.3 76.3 %copy-start.12 = (bf16[128,512]{1,0:T(8,128)(2,1)S(1)}, bf16[128,512]{1,0:T(8,128)(2,1)}, u32[]{:S(2)}) copy-start(bf16[128,512]{1,0:T(8,128)(2,1)} %param.26) | copy-start | bytes 393220
  11.3 109.1 %all-gather.8.cloned.1.call-start = ((), (), s32[]{:S(2)}) async-start(), calls=%async_computation.4 | async-start | bytes 1310720 | tf_op jit(solution)/shard_map/all_gather | solution.py:81
  12.1 168.7 %reduce-scatter.3.cloned.1.call-start = ((), (), s32[]{:S(2)}) async-start(), calls=%async_computation.5 | async-start | bytes 5734400 | tf_op jit(solution)/shard_map/reduce_scatter | solution.py:92
  109.0 4.7 %copy-start.4 = (bf16[640,4,1,128]{0,3,2,1:T(8,128)(2,1)}, bf16[640,4,1,128]{0,3,2,1:T(8,128)(2,1)S(1)}, u32[]{:S(2)}) copy-start(bf16[640,4,1,128]{0,3,2,1:T(8,128)(2,1)S(1)} %constant_dynamic-slice_fusion) | copy-start | bytes 1966084
  118.6 1.8 copy-start.5
  120.4 4.7 %copy-start.6 = (bf16[512,512]{1,0:T(8,128)(2,1)S(1)}, bf16[512,512]{1,0:T(8,128)(2,1)}, u32[]{:S(2)}) copy-start(bf16[512,512]{1,0:T(8,128)(2,1)} %all_gather.46) | copy-start | bytes 1572868
  126.6 2.0 copy-start.3
  126.6 2.1 copy-start.7
  126.6 55.3 %copy-start.16 = (f32[512]{0:T(512)S(1)}, f32[512]{0:T(512)}, u32[]{:S(2)}) copy-start(f32[512]{0:T(512)} %param.28) | copy-start | bytes 6148
  126.6 126.7 %all-gather.10.cloned.1.call-start = ((), (), s32[]{:S(2)}) async-start(), calls=%async_computation.6 | async-start | bytes 1638400 | tf_op jit(solution)/shard_map/all_gather | solution.py:196
  211.8 1.7 copy-start.1
  215.4 1.6 copy-start.2
  217.0 2.1 copy-start.17
  219.1 1.2 copy-start.15
  219.1 2.8 copy-start.14
  219.1 4.4 %copy-start.13 = (bf16[512,128]{1,0:T(8,128)(2,1)S(1)}, bf16[512,128]{1,0:T(8,128)(2,1)}, u32[]{:S(2)}) copy-start(bf16[512,128]{1,0:T(8,128)(2,1)} %param.32) | copy-start | bytes 393220
  221.3 61.5 %all-gather.12.cloned.1.call-start = ((), (), s32[]{:S(2)}) async-start(), calls=%async_computation.7 | async-start | bytes 1310720 | tf_op jit(solution)/shard_map/all_gather | solution.py:210
  221.9 70.7 %reduce-scatter.5.cloned.1.call-start = ((), (), s32[]{:S(2)}) async-start(), calls=%async_computation.8 | async-start | bytes 983040 | tf_op jit(solution)/shard_map/reduce_scatter | solution.py:212
  222.0 15.9 %collective-permute-start = (bf16[2,512]{1,0:T(2,128)(2,1)S(1)}, bf16[2,512]{1,0:T(2,128)(2,1)S(1)}, u32[]{:S(2)}, u32[]{:S(2)}) collective-permute-start(bf16[2,512]{1,0:T(2,128)(2,1)S(1)} %slice.44), channel_id=1, source_target_pairs={{0,8},{8,16},{16,24},{1,9},{9,17},{17,25},{2,10},{10,18},{18,26},{... | collective-permute-start | bytes 6152 | tf_op jit(solution)/shard_map/ppermute | solution.py:18
Sparse Core Ops, SparseCore 0:
  11.5 42.1 all-gather.5
  55.2 39.4 all-gather.7
  126.7 54.0 reduce-scatter.2
  221.4 30.0 all-gather.9
  253.0 29.7 all-gather.11
  286.2 6.3 reduce-scatter.4
